TPU v7x, 512 devices: a whole 4x8x8 slice. The times are simulated.
512 devices in a mesh: sp: 32 (over z, x), tp: 16 (over y, core).
Axes of the slice: x: 4, y: 8, z: 8, core: 2. Of those that a mesh axis runs over, the one named last changes fastest.
Arguments:
- outer_gate: bfloat16 [512, 12288], P('tp', 'sp'), may hold values from -6 to 6
- inner_gate: bfloat16 [512, 12288], P('tp', 'sp'), may hold values from -6 to 6
- conv_input: bfloat16 [512, 12288], P('tp', 'sp'), may hold values from -6 to 6
- conv_taps: bfloat16 [3, 512], P(None, 'tp'), may hold values from -3.5 to 3.5
- mix_weight: bfloat16 [512, 2048], P(None, 'tp'), may hold values from -0.25 to 0.25
- residual: bfloat16 [12288, 2048], P('sp', 'tp'), may hold values from -24 to 24
- norm_gain: bfloat16 [2048], P('tp'), may hold values from 0.099609375 to 1.8984375
- routes: int32 [12288, 2], P('sp'), may hold values from 0 to 63, all different within a row; in each aligned block of 384 rows (0 to 383, 384 to 767, ...) at most 24 rows name the same one
- route_scores: float32 [12288, 2], P('sp'), may hold values from 0.05 to 1
- expert_gate: bfloat16 [64, 2048, 2048], P('sp', None, 'tp'), may hold values from -0.125 to 0.125
- expert_up: bfloat16 [64, 2048, 2048], P('sp', None, 'tp'), may hold values from -0.125 to 0.125
- expert_down: bfloat16 [64, 2048, 2048], P('sp', None, 'tp'), may hold values from -0.125 to 0.125
- shared_gate: bfloat16 [2048, 512], P(None, 'tp'), may hold values from -0.125 to 0.125
- shared_up: bfloat16 [2048, 512], P(None, 'tp'), may hold values from -0.125 to 0.125
- shared_down: bfloat16 [512, 2048], P(None, 'tp'), may hold values from -0.25 to 0.25
Outputs:
- layer_out: bfloat16 [12288, 2048], P('sp', 'tp')
Inputs may be any that keep to these rules, and one draw needn't show every extreme that they name: `routes`: within the rows of one index of sp (384 tokens), no expert is named by more than 24 of the token and choice pairs, a bound that some block reaches; the experts of one token differ.
All inputs are finite; a program needn't handle non-finite values.
Results may differ from a plain program's by a relative error of at most 0.014.
Values may be sent and summed in bfloat16 or wider, within the bound.
No kernel may reach another device: no remote copies, remote signals or barrier semaphores. Data moves between devices by JAX's collectives and lax.ppermute only.
A program may use at most 64 MiB of HBM per device.

v0:
```python
import jax
import jax.numpy as jnp
from jax import lax
from jax.sharding import PartitionSpec as P

D = 2048
epsilon = 1e-06
routed_scale = 2.5


def extended(array, sides, width):
    for axis, dim in sides:
        peers, length = (lax.axis_size(axis), array.shape[dim])
        up = [(i, (i + 1) % peers) for i in range(peers - 1)]
        down = [(j, i) for i, j in up]
        last = lax.slice_in_dim(array, length - width, length, axis=dim)
        first = lax.slice_in_dim(array, 0, width, axis=dim)
        before = lax.ppermute(last, axis, up)
        after = lax.ppermute(first, axis, down)
        array = jnp.concatenate([before, array, after], axis=dim)
    return array


def copy_for_each(array, axis):
    peers = lax.axis_size(axis)
    return lax.all_to_all(
        jnp.broadcast_to(array[None], (peers, *array.shape)), axis, 0, 0, tiled=True
    )


def taken_together(array, axis):
    return copy_for_each(array, axis).sum(axis=0)


def slot_tables(routes_block, expert_count, capacity):
    count_rows, top_count = routes_block.shape
    flat_route = routes_block.reshape(-1)
    onehot = (flat_route[:, None] == jnp.arange(expert_count, dtype=jnp.int32)[None, :]).astype(
        jnp.int32
    )
    before = jnp.cumsum(onehot, axis=0) - onehot
    position = jnp.sum(before * onehot, axis=1)
    slot_index = flat_route * capacity + position
    token_ids = jnp.arange(count_rows * top_count, dtype=jnp.int32) // top_count
    owners = jnp.full((expert_count * capacity,), -1, jnp.int32).at[slot_index].set(token_ids)
    return (slot_index.reshape(count_rows, top_count), owners)


def local(
    outer_gate,
    inner_gate,
    conv_input,
    conv_taps,
    mix_weight,
    residual,
    norm_gain,
    routes,
    route_scores,
    expert_gate,
    expert_up,
    expert_down,
    shared_gate,
    shared_up,
    shared_down,
):
    product = (inner_gate.astype(jnp.float32) * conv_input.astype(jnp.float32)).astype(jnp.bfloat16)
    padded = extended(product, (("sp", 1),), 1).astype(jnp.float32)
    kernel = conv_taps.astype(jnp.float32)
    filtered = (
        kernel[0][:, None] * padded[:, :-2]
        + kernel[1][:, None] * padded[:, 1:-1]
        + kernel[2][:, None] * padded[:, 2:]
    )
    mixed = (outer_gate.astype(jnp.float32) * filtered).astype(jnp.bfloat16)
    token_count = mixed.shape[1]
    rows_w = mix_weight
    projected = lax.dot_general(
        lax.all_gather(mixed, "tp", axis=0, tiled=True),
        rows_w,
        (((0,), (0,)), ((), ())),
        preferred_element_type=jnp.float32,
    )
    stream = (residual.astype(jnp.float32) + projected).astype(jnp.bfloat16)
    levels = stream.astype(jnp.float32)
    squares = taken_together(jnp.sum(levels * levels, axis=1), "tp")
    inverse_rms = lax.rsqrt(squares / D + epsilon)
    normed = (levels * inverse_rms[:, None] * norm_gain.astype(jnp.float32)).astype(jnp.bfloat16)
    whole_rows = lax.all_gather(normed, "tp", axis=1, tiled=True)
    shared_act = (
        jax.nn.silu(jnp.dot(whole_rows, shared_gate, preferred_element_type=jnp.float32))
        * jnp.dot(whole_rows, shared_up, preferred_element_type=jnp.float32)
    ).astype(jnp.bfloat16)
    rows_w = shared_down
    shared_out = jnp.dot(
        lax.all_gather(shared_act, "tp", axis=1, tiled=True),
        rows_w,
        preferred_element_type=jnp.float32,
    )
    group_count = lax.axis_size("sp")
    local_experts = expert_gate.shape[0]
    expert_count = local_experts * group_count
    capacity = 2 * token_count * routes.shape[1] // expert_count
    slot_index, owners = slot_tables(routes, expert_count, capacity)
    filled = owners >= 0
    source_ids = jnp.maximum(owners, 0)
    outgoing = jnp.where(filled[:, None], normed[source_ids], jnp.zeros((), jnp.bfloat16)).reshape(
        group_count, local_experts * capacity, -1
    )
    sliced = lax.all_to_all(outgoing, "sp", split_axis=0, concat_axis=1, tiled=True)
    received = lax.all_gather(sliced, "tp", axis=2, tiled=True)
    arrived = (
        received.reshape(group_count, local_experts, capacity, -1)
        .transpose(1, 0, 2, 3)
        .reshape(local_experts, group_count * capacity, -1)
    )
    gate_act = jnp.einsum("erd,edf->erf", arrived, expert_gate, preferred_element_type=jnp.float32)
    up_act = jnp.einsum("erd,edf->erf", arrived, expert_up, preferred_element_type=jnp.float32)
    hidden = (jax.nn.silu(gate_act) * up_act).astype(jnp.bfloat16)
    rows_w = expert_down
    expert_rows = jnp.einsum(
        "erf,efd->erd",
        lax.all_gather(hidden, "tp", axis=2, tiled=True),
        rows_w,
        preferred_element_type=jnp.float32,
    ).astype(jnp.bfloat16)
    feature_count = expert_rows.shape[2]
    regrouped = (
        expert_rows.reshape(local_experts, group_count, capacity, feature_count)
        .transpose(1, 0, 2, 3)
        .reshape(1, group_count * local_experts * capacity, feature_count)
    )
    returned = lax.all_to_all(regrouped, "sp", split_axis=1, concat_axis=0, tiled=True)
    flat_rows = returned.reshape(expert_count * capacity, feature_count)
    picked = flat_rows[slot_index].astype(jnp.float32)
    weights = route_scores / jnp.sum(route_scores, axis=1, keepdims=True) * routed_scale
    routed = jnp.einsum("tk,tkd->td", weights, picked)
    return (levels + routed + shared_out).astype(jnp.bfloat16)


def solution(mesh):
    in_specs = (
        P("tp", "sp"),
        P("tp", "sp"),
        P("tp", "sp"),
        P(None, "tp"),
        P(None, "tp"),
        P("sp", "tp"),
        P("tp"),
        P("sp", None),
        P("sp", None),
        P("sp", None, "tp"),
        P("sp", None, "tp"),
        P("sp", None, "tp"),
        P(None, "tp"),
        P(None, "tp"),
        P(None, "tp"),
    )
    out_specs = P("sp", "tp")
    return jax.shard_map(local, mesh=mesh, in_specs=in_specs, out_specs=out_specs, check_vma=False)
```

profile of v0, /device:TPU:1, one launch (start us, length us, event | category | flops | bytes accessed | tf_op | source)
XLA Modules:
  0.0 281.1 jit_solution(13468960967642711488)
XLA Ops:
  6.5 0.9 multiply_convert_fusion.1
  7.4 0.1 fusion.19
  7.5 3.9 %collective-permute-start = (bf16[32,1]{1,0:T(8,128)(2,1)S(1)}, bf16[32,1]{1,0:T(8,128)(2,1)S(1)}, u32[]{:S(2)}, u32[]{:S(2)}) collective-permute-start(bf16[32,1]{1,0:T(8,128)(2,1)S(1)} %get-tuple-element.7), channel_id=1, source_target_pairs={{0,16},{16,32},{32,48},{48,64},{64,80},{80,96},{96,112},{112,128},... | collective-permute-start | bytes 200 | tf_op jit(solution)/shard_map/ppermute | solution.py:18
  11.4 1.3 collective-permute-start.1
  12.7 0.8 copy.64
  13.5 0.1 eq.29
  13.7 0.1 eq.25
  13.9 1.8 reduce-window.6
  15.7 0.3 slice_reduce_fusion
  16.0 0.1 fusion.7
  16.1 0.2 reduce_sum.45
  16.3 0.2 mul.110
  16.5 3.4 %scatter_custom_fusion = s32[1536]{0:T(1024)S(1)} fusion(s32[768]{0:T(1024)S(1)} %fusion.18, s32[768]{0:T(1024)S(1)} %add_select_fusion, s32[]{:T(128)} %constant.23.clone.1), kind=kCustom, calls=%fused_computation.49 | custom fusion | bytes 6148 | tf_op jit(solution)/shard_map/scatter | solution.py:45
  19.9 0.7 convert_element_type.58
  20.6 1.0 copy.63
  21.6 0.1 maximum_convert_fusion
  21.7 0.8 fusion.11
  22.6 19.5 %all_gather.15 = bf16[512,384]{1,0:T(8,128)(2,1)S(1)} all-gather(bf16[32,384]{1,0:T(8,128)(2,1)S(1)} %fusion.11), channel_id=1, replica_groups=mesh['sp'=32,'tp'=16] {'tp'}, dimensions={0}, use_global_device_ids=true | all-gather | bytes 417792 | tf_op jit(solution)/shard_map/all_gather | solution.py:78
  42.0 1.2 multiply_reduce_fusion.1
  43.2 0.6 broadcast_in_dim.38
  43.9 4.5 %all-to-all-start = ((f32[16,1,384]{2,1,0:T(1,128)}), f32[16,1,384]{2,1,0:T(1,128)S(1)}, u32[]{:S(2)}, u32[]{:S(2)}) async-start(f32[16,1,384]{2,1,0:T(1,128)} %broadcast_in_dim.38), calls=%async_computation | async-start | bytes 49152 | tf_op jit(solution)/shard_map/all_to_all | solution.py:26
  48.3 0.0 all-gather.4.cloned.1.call-start
  48.4 0.7 convert_element_type.68
  49.1 0.1 broadcast_in_dim.36
  49.2 6.6 %all-to-all-done = f32[16,1,384]{2,1,0:T(1,128)S(1)} async-done(((f32[16,1,384]{2,1,0:T(1,128)}), f32[16,1,384]{2,1,0:T(1,128)S(1)}, u32[]{:S(2)}, u32[]{:S(2)}) %all-to-all-start) | async-done | bytes 24608 | tf_op jit(solution)/shard_map/all_to_all | solution.py:26
  55.8 0.1 multiply_convert_fusion
  55.9 0.0 copy-start.1
  55.9 0.1 copy.69
  56.0 3.2 %gather_fusion = bf16[1536,128]{1,0:T(8,128)(2,1)S(1)} fusion(bf16[384,128]{1,0:T(8,128)(2,1)S(1)} %copy.69, s32[2048]{0:T(1024)S(1)} %pad_clamp_fusion), kind=kCustom, calls=%fused_computation | custom fusion | bytes 792576 | tf_op jit(solution)/shard_map/gather | solution.py:106
  59.2 0.3 broadcast_select_fusion
  59.5 28.7 %all_to_all.27 = bf16[32,48,128]{2,1,0:T(8,128)(2,1)} all-to-all(bf16[32,48,128]{2,1,0:T(8,128)(2,1)S(1)} %broadcast_select_fusion), channel_id=1, replica_groups=mesh['sp'=32,'tp'=16] {'sp'}, dimensions={0} | all-to-all | bytes 786432 | tf_op jit(solution)/shard_map/all_to_all | solution.py:109
  88.1 0.0 all-gather.4.cloned.1.call-update
  88.2 0.0 all-gather.6.cloned.1.call-start
  88.2 52.3 %all-gather.4.cloned.1.call-done = bf16[1,1536,2048]{2,1,0:T(8,128)(2,1)} async-done(((bf16[1,1536,128]{2,1,0:T(8,128)(2,1)}), bf16[1,1536,2048]{2,1,0:T(8,128)(2,1)}) %all-gather.4.cloned.1.call-update) | async-done | bytes 6291472 | tf_op jit(solution)/shard_map/all_gather | solution.py:110
  140.5 3.4 %copy.70 = bf16[2,32,24,2048]{3,2,1,0:T(8,128)(2,1)S(1)} copy(bf16[2,32,24,2048]{3,2,0,1:T(8,128)(2,1)} %bitcast.62) | data formatting | bytes 12582912 | tf_op jit(solution)/shard_map/transpose | solution.py:113
  143.9 0.0 copy-start.6
  143.9 1.8 fusion.20
  145.7 0.0 copy-start.7
  145.7 2.5 fusion
  148.3 0.0 all-gather.6.cloned.1.call-update
  148.3 0.2 all-gather.8.cloned.1.call-start
  148.5 0.5 all-gather.8.cloned.1.call-update
  149.1 0.1 reshape.110
  149.3 0.0 copy-start.2
  149.3 58.0 %all-gather.6.cloned.1.call-done = bf16[2,768,2048]{2,1,0:T(8,128)(2,1)} async-done(((bf16[2,768,128]{2,1,0:T(8,128)(2,1)}), bf16[2,768,2048]{2,1,0:T(8,128)(2,1)}) %all-gather.6.cloned.1.call-update) | async-done | bytes 6291472 | tf_op jit(solution)/shard_map/all_gather | solution.py:122
  207.3 4.6 %convolution_convert_fusion = bf16[2,768,128]{2,1,0:T(8,128)(2,1)S(1)} fusion(bf16[2,768,2048]{2,1,0:T(8,128)(2,1)} %all-gather.6.cloned.1.call-done, bf16[2,2048,128]{2,1,0:T(8,128)(2,1)S(1)} %copy-done.7), kind=kOutput, calls=%fused_computation.5 | convolution fusion | flops 805502976 | bytes 7733248 | tf_op jit(solution)/shard_map/erf,efd->erd/dot_general | solution.py:120
  211.9 6.1 %copy.88 = bf16[1,1536,128]{2,0,1:T(2,128)(2,1)S(1)} copy(bf16[1,1536,128]{2,1,0:T(8,128)(2,1)S(1)} %bitcast.67) | data formatting | bytes 786432 | tf_op jit(solution)/shard_map/reshape | solution.py:130
  218.1 0.6 broadcast.89
  218.7 8.8 %reduce.7 = bf16[1536,128]{1,0:T(8,128)(2,1)S(1)} reduce(bf16[1536,1,128]{2,1,0:T(2,128)(2,1)S(1)} %bitcast.63, bf16[]{:T(256)} %broadcast.89), dimensions={1}, to_apply=%bitcast.56.reduce_sub_computation | reduce | bytes 786434
  227.5 0.8 reshape.133
  228.3 9.9 %all-to-all-start.2 = ((bf16[32,2,3072]{2,1,0:T(2,128)(2,1)}), bf16[32,2,3072]{2,1,0:T(2,128)(2,1)S(1)}, u32[]{:S(2)}, u32[]{:S(2)}) async-start(bf16[32,2,3072]{2,1,0:T(2,128)(2,1)} %reshape.133), calls=%async_computation.2 | async-start | bytes 786432 | tf_op jit(solution)/shard_map/all_to_all | solution.py:132
  238.3 0.1 copy.82
  238.4 11.7 %all-gather.8.cloned.1.call-done = bf16[384,2048]{0,1:T(8,128)(2,1)} async-done(((bf16[384,128]{0,1:T(8,128)(2,1)}), bf16[384,2048]{0,1:T(8,128)(2,1)}) %all-gather.8.cloned.1.call-update) | async-done | bytes 1572880 | tf_op jit(solution)/shard_map/all_gather | solution.py:88
  250.1 1.7 fusion.21
  251.9 0.0 copy-done.2
  251.9 1.8 fusion.4
  253.7 16.9 %all_gather.19 = bf16[384,512]{0,1:T(8,128)(2,1)S(1)} all-gather(bf16[384,32]{0,1:T(8,128)(2,1)S(1)} %fusion.4), channel_id=1, replica_groups=mesh['sp'=32,'tp'=16] {'tp'}, dimensions={1}, use_global_device_ids=true | all-gather | bytes 417792 | tf_op jit(solution)/shard_map/all_gather | solution.py:95
  270.5 0.3 reshape.134
  270.9 0.1 copy.87
  270.9 1.9 gather_fusion.1
  272.8 0.6 multiply_reduce_fusion
  273.4 0.1 copy.78
  273.5 0.3 fusion.3
  273.8 0.8 copy.74
  (29 shorter events, 0.3 us)
Async XLA Ops:
  6.5 137.4 %copy-start = (bf16[2,2048,128]{2,1,0:T(8,128)(2,1)S(1)}, bf16[2,2048,128]{2,1,0:T(8,128)(2,1)}, u32[]{:S(2)}) copy-start(bf16[2,2048,128]{2,1,0:T(8,128)(2,1)} %param.24) | copy-start | bytes 3145732
  7.5 14.2 %collective-permute-start = (bf16[32,1]{1,0:T(8,128)(2,1)S(1)}, bf16[32,1]{1,0:T(8,128)(2,1)S(1)}, u32[]{:S(2)}, u32[]{:S(2)}) collective-permute-start(bf16[32,1]{1,0:T(8,128)(2,1)S(1)} %get-tuple-element.7), channel_id=1, source_target_pairs={{0,16},{16,32},{32,48},{48,64},{64,80},{80,96},{96,112},{112,128},... | collective-permute-start | bytes 200 | tf_op jit(solution)/shard_map/ppermute | solution.py:18
  11.4 10.2 %collective-permute-start.1 = (bf16[32,1]{1,0:T(8,128)(2,1)S(1)}, bf16[32,1]{1,0:T(8,128)(2,1)S(1)}, u32[]{:S(2)}, u32[]{:S(2)}) collective-permute-start(bf16[32,1]{1,0:T(8,128)(2,1)S(1)} %get-tuple-element.8), channel_id=1, source_target_pairs={{16,0},{32,16},{48,32},{64,48},{80,64},{96,80},{112,96},{128,112},... | collective-permute-start | bytes 200 | tf_op jit(solution)/shard_map/ppermute | solution.py:19
  43.9 11.9 %all-to-all-start = ((f32[16,1,384]{2,1,0:T(1,128)}), f32[16,1,384]{2,1,0:T(1,128)S(1)}, u32[]{:S(2)}, u32[]{:S(2)}) async-start(f32[16,1,384]{2,1,0:T(1,128)} %broadcast_in_dim.38), calls=%async_computation | async-start | bytes 49152 | tf_op jit(solution)/shard_map/all_to_all | solution.py:26
  48.3 92.2 %all-gather.4.cloned.1.call-start = ((), (), s32[]{:S(2)}) async-start(), calls=%async_computation.3 | async-start | bytes 6684672 | tf_op jit(solution)/shard_map/all_gather | solution.py:110
  55.9 88.0 %copy-start.1 = (bf16[384,128]{0,1:T(8,128)(2,1)}, bf16[384,128]{0,1:T(8,128)(2,1)S(1)}, u32[]{:S(2)}) copy-start(bf16[384,128]{0,1:T(8,128)(2,1)S(1)} %multiply_convert_fusion) | copy-start | bytes 294916
  88.2 119.1 %all-gather.6.cloned.1.call-start = ((), (), s32[]{:S(2)}) async-start(), calls=%async_computation.4 | async-start | bytes 6684672 | tf_op jit(solution)/shard_map/all_gather | solution.py:122
  143.9 1.8 copy-start.6
  145.7 3.3 %copy-start.5 = (f32[384,2]{0,1:T(2,128)S(1)}, f32[384,2]{0,1:T(2,128)}, u32[]{:S(2)}) copy-start(f32[384,2]{0,1:T(2,128)} %param.23) | copy-start | bytes 9220
  145.7 61.6 %copy-start.7 = (bf16[2,2048,128]{2,1,0:T(8,128)(2,1)S(1)}, bf16[2,2048,128]{2,1,0:T(8,128)(2,1)}, u32[]{:S(2)}) copy-start(bf16[2,2048,128]{2,1,0:T(8,128)(2,1)} %param.26) | copy-start | bytes 3145732
  148.3 101.8 %all-gather.8.cloned.1.call-start = ((), (), s32[]{:S(2)}) async-start(), calls=%async_computation.5 | async-start | bytes 1671168 | tf_op jit(solution)/shard_map/all_gather | solution.py:88
  149.2 100.9 %copy-start.3 = (bf16[2048,32]{0,1:T(8,128)(2,1)S(1)}, bf16[2048,32]{0,1:T(8,128)(2,1)}, u32[]{:S(2)}) copy-start(bf16[2048,32]{0,1:T(8,128)(2,1)} %param.27) | copy-start | bytes 393220
  149.3 102.6 %copy-start.2 = (bf16[2048,32]{0,1:T(8,128)(2,1)S(1)}, bf16[2048,32]{0,1:T(8,128)(2,1)}, u32[]{:S(2)}) copy-start(bf16[2048,32]{0,1:T(8,128)(2,1)} %param.28) | copy-start | bytes 393220
  218.1 55.5 %copy-start.4 = (bf16[512,128]{1,0:T(8,128)(2,1)S(1)}, bf16[512,128]{1,0:T(8,128)(2,1)}, u32[]{:S(2)}) copy-start(bf16[512,128]{1,0:T(8,128)(2,1)} %param.29) | copy-start | bytes 393220
  228.3 42.2 %all-to-all-start.2 = ((bf16[32,2,3072]{2,1,0:T(2,128)(2,1)}), bf16[32,2,3072]{2,1,0:T(2,128)(2,1)S(1)}, u32[]{:S(2)}, u32[]{:S(2)}) async-start(bf16[32,2,3072]{2,1,0:T(2,128)(2,1)} %reshape.133), calls=%async_computation.2 | async-start | bytes 786432 | tf_op jit(solution)/shard_map/all_to_all | solution.py:132
Sparse Core Ops, SparseCore 0:
  88.3 52.1 all-gather.3
  148.4 58.8 all-gather.5
  209.4 40.6 all-gather.7
where the time goes:
time: 282 us; the launch traced here: 281 us
  waiting for transfers between devices  129 us (46%)
  blocking collectives  65 us (23%)
  local copies, waits for them, and re-layouts  24.6 us (9%)
  starting transfers between devices  19.9 us (7%)
  other arithmetic  15 us (5%)
  matrix products  13.9 us (5%)
  between operations  13.5 us (5%)
    all_gather x1, waiting for transfers between devices, local(): lax.all_gather(hidden, 'tp', axis=2, tiled=True)  58 us
    all_gather x1, waiting for transfers between devices, local(): received = lax.all_gather(sliced, 'tp', axis=2, tiled=True)  52.3 us
    all_to_all x1, blocking collectives, local(): lax.all_to_all(outgoing, 'sp', split_axis=0, concat_axis=1, tiled=True)  28.7 us
    all_gather x1, blocking collectives, local(): lax.all_gather(mixed, 'tp', axis=0, tiled=True)  19.5 us
    all_gather x1, blocking collectives, local(): lax.all_gather(shared_act, 'tp', axis=1, tiled=True)  16.9 us
    all_gather x1, waiting for transfers between devices, local(): whole_rows = lax.all_gather(normed, 'tp', axis=1, tiled=True)  11.7 us
    all_to_all x1, starting transfers between devices, local(): lax.all_to_all(regrouped, 'sp', split_axis=1, concat_axis=0, tiled=True)  9.9 us
    unnamed x2, other arithmetic  9.43 us
  transfers between devices with their start and end apart: 7, of which 4 were waited for; matrix products, arithmetic and copies ran while one was open for 12% of the time, Pallas kernels for 0%

commit v1 on v0

--- a/solution.py
+++ b/solution.py
@@ -1,11 +1,42 @@
+import functools
 import jax
 import jax.numpy as jnp
 from jax import lax
 from jax.sharding import PartitionSpec as P
+from jax.lax import axis_index, axis_size, ppermute
 
 D = 2048
 epsilon = 1e-06
 routed_scale = 2.5
+
+
+def expand_sums_all(block_here, axis_key):
+    long_array = axis_size(axis_key)
+    items = []
+    fresh, q_next, near = (long_array, axis_index(axis_key), block_here.shape[0])
+    for k0, dev_i in enumerate(block_here.shape):
+        items.append(dev_i * fresh if k0 == 0 else dev_i)
+    local_part = jnp.zeros(items, block_here.dtype)
+    g_now = lax.dynamic_update_slice_in_dim(local_part, block_here, q_next * near, axis=0)
+    ready = mixed_arr = block_here
+    for t in range(1, fresh // 2 + 1):
+        by_rank = []
+        for k0 in range(fresh):
+            by_rank.append((k0, (k0 + 1) % fresh))
+        ready = ppermute(ready, axis_name=axis_key, perm=by_rank)
+        g_now = lax.dynamic_update_slice_in_dim(g_now, ready, (q_next - t) % fresh * near, axis=0)
+        if 2 * t < fresh:
+            so_far_all = []
+            for k0 in range(fresh):
+                so_far_all.append((k0, (k0 - 1) % fresh))
+            mixed_arr = ppermute(mixed_arr, axis_key, perm=so_far_all)
+            g_now = lax.dynamic_update_slice_in_dim(
+                g_now, mixed_arr, (q_next + t) % fresh * near, axis=0
+            )
+    return g_now
+
+
+scan_slices_on = functools.partial(expand_sums_all, axis_key="tp")
 
 
 def extended(array, sides, width):
@@ -75,10 +106,7 @@
     token_count = mixed.shape[1]
     rows_w = mix_weight
     projected = lax.dot_general(
-        lax.all_gather(mixed, "tp", axis=0, tiled=True),
-        rows_w,
-        (((0,), (0,)), ((), ())),
-        preferred_element_type=jnp.float32,
+        scan_slices_on(mixed), rows_w, (((0,), (0,)), ((), ())), preferred_element_type=jnp.float32
     )
     stream = (residual.astype(jnp.float32) + projected).astype(jnp.bfloat16)
     levels = stream.astype(jnp.float32)

time: 282 us -> 301 us (1.067)
  starting transfers between devices: 19.9 us -> 48.7 us
  blocking collectives: 65 us -> 45.5 us
  waiting for transfers between devices: 129 us -> 138 us
    ppermute x0 -> x15, starting transfers between devices: none -> 25.7 us  [the longest x7 23.4 us: expand_sums_all(): mixed_arr = ppermute(mixed_arr, axis_key, perm=so_far_all)]
    all_gather x1 -> x0, blocking collectives: 19.5 us -> none  [local(): lax.all_gather(mixed, 'tp', axis=0, tiled=True)]
    ppermute x0 -> x15, waiting for transfers between devices: none -> 9.22 us  [the longest x8 8.18 us: expand_sums_all(): ready = ppermute(ready, axis_name=axis_key, perm=by_rank)]
    all_to_all x1, starting transfers between devices: 4.49 us -> 7.64 us  [copy_for_each(): lax.all_to_all(jnp.broadcast_to(array[None], (peers, *array.shape)), axis...]
  transfers between devices with their start and end apart: 7 -> 22, of which waited for: 4 -> 17; matrix products, arithmetic and copies ran while one was open for 12% -> 11% of each run, Pallas kernels for 0% -> 0%
where the time goes in v1:
time: 301 us; the launch traced here: 300 us
  waiting for transfers between devices  138 us (46%)
  starting transfers between devices  48.7 us (16%)
  blocking collectives  45.5 us (15%)
  local copies, waits for them, and re-layouts  24.8 us (8%)
  other arithmetic  15 us (5%)
  matrix products  13.9 us (5%)
  between operations  13.6 us (5%)
    all_gather x1, waiting for transfers between devices, local(): lax.all_gather(hidden, 'tp', axis=2, tiled=True)  58 us
    all_gather x1, waiting for transfers between devices, local(): received = lax.all_gather(sliced, 'tp', axis=2, tiled=True)  52.3 us
    all_to_all x1, blocking collectives, local(): lax.all_to_all(outgoing, 'sp', split_axis=0, concat_axis=1, tiled=True)  28.7 us
    ppermute x7, starting transfers between devices, expand_sums_all(): mixed_arr = ppermute(mixed_arr, axis_key, perm=so_far_all)  23.4 us
    all_gather x1, blocking collectives, local(): lax.all_gather(shared_act, 'tp', axis=1, tiled=True)  16.9 us
    all_gather x1, waiting for transfers between devices, local(): whole_rows = lax.all_gather(normed, 'tp', axis=1, tiled=True)  11.8 us
    all_to_all x1, starting transfers between devices, local(): lax.all_to_all(regrouped, 'sp', split_axis=1, concat_axis=0, tiled=True)  9.9 us
    unnamed x2, other arithmetic  9.37 us
  transfers between devices with their start and end apart: 22, of which 17 were waited for; matrix products, arithmetic and copies ran while one was open for 11% of the time, Pallas kernels for 0%

profile of v1, /device:TPU:1, one launch (start us, length us, event | category | flops | bytes accessed | tf_op | source)
XLA Modules:
  0.0 300.1 jit_solution(16814710883520530095)
XLA Ops:
  6.5 0.9 multiply_convert_fusion.1
  7.5 3.9 %collective-permute-start = (bf16[32,1]{1,0:T(8,128)(2,1)S(1)}, bf16[32,1]{1,0:T(8,128)(2,1)S(1)}, u32[]{:S(2)}, u32[]{:S(2)}) collective-permute-start(bf16[32,1]{1,0:T(8,128)(2,1)S(1)} %get-tuple-element.9), channel_id=1, source_target_pairs={{0,16},{16,32},{32,48},{48,64},{64,80},{80,96},{96,112},{112,128},... | collective-permute-start | bytes 200 | tf_op jit(solution)/shard_map/ppermute | solution.py:49
  11.4 1.3 collective-permute-start.1
  12.7 0.8 copy.64
  13.5 0.1 eq.45
  13.8 0.7 convert_element_type.58
  14.5 1.8 reduce-window.6
  16.4 0.3 slice_reduce_fusion
  16.8 0.2 reduce_sum.45
  17.0 0.2 mul.174
  17.2 3.4 %scatter_custom_fusion = s32[1536]{0:T(1024)S(1)} fusion(s32[768]{0:T(1024)S(1)} %fusion.18, s32[768]{0:T(1024)S(1)} %add_select_fusion, s32[]{:T(128)} %constant.129.clone.1), kind=kCustom, calls=%fused_computation.49 | custom fusion | bytes 6148 | tf_op jit(solution)/shard_map/scatter | solution.py:76
  20.8 0.9 constant_dynamic-update-slice_fusion.15
  21.6 2.1 collective-permute-start.2
  23.8 2.1 collective-permute-start.3
  25.9 1.0 copy.63
  27.0 3.3 %collective-permute-start.5 = (bf16[32,384]{1,0:T(8,128)(2,1)S(1)}, bf16[32,384]{1,0:T(8,128)(2,1)S(1)}, u32[]{:S(2)}, u32[]{:S(2)}) collective-permute-start(bf16[32,384]{1,0:T(8,128)(2,1)S(1)} %collective-permute-done.3), channel_id=1, source_target_pairs={{0,15},{1,0},{2,1},{3,2},{4,3},{5,4},{6,5},{7,6},{8,7},{9,8},{10,9... | collective-permute-start | bytes 73736 | tf_op jit(solution)/shard_map/ppermute | solution.py:32
  30.3 0.7 collective-permute-done.4
  31.0 0.2 collective-permute-done.5
  31.2 3.6 %collective-permute-start.7 = (bf16[32,384]{1,0:T(8,128)(2,1)S(1)}, bf16[32,384]{1,0:T(8,128)(2,1)S(1)}, u32[]{:S(2)}, u32[]{:S(2)}) collective-permute-start(bf16[32,384]{1,0:T(8,128)(2,1)S(1)} %collective-permute-done.5), channel_id=1, source_target_pairs={{0,15},{1,0},{2,1},{3,2},{4,3},{5,4},{6,5},{7,6},{8,7},{9,8},{10,9... | collective-permute-start | bytes 73736 | tf_op jit(solution)/shard_map/ppermute | solution.py:32
  34.8 0.6 collective-permute-done.6
  35.4 0.2 collective-permute-done.7
  35.6 3.6 %collective-permute-start.9 = (bf16[32,384]{1,0:T(8,128)(2,1)S(1)}, bf16[32,384]{1,0:T(8,128)(2,1)S(1)}, u32[]{:S(2)}, u32[]{:S(2)}) collective-permute-start(bf16[32,384]{1,0:T(8,128)(2,1)S(1)} %collective-permute-done.7), channel_id=1, source_target_pairs={{0,15},{1,0},{2,1},{3,2},{4,3},{5,4},{6,5},{7,6},{8,7},{9,8},{10,9... | collective-permute-start | bytes 73736 | tf_op jit(solution)/shard_map/ppermute | solution.py:32
  39.3 0.6 collective-permute-done.8
  39.9 0.2 collective-permute-done.9
  40.1 3.6 %collective-permute-start.11 = (bf16[32,384]{1,0:T(8,128)(2,1)S(1)}, bf16[32,384]{1,0:T(8,128)(2,1)S(1)}, u32[]{:S(2)}, u32[]{:S(2)}) collective-permute-start(bf16[32,384]{1,0:T(8,128)(2,1)S(1)} %collective-permute-done.9), channel_id=1, source_target_pairs={{0,15},{1,0},{2,1},{3,2},{4,3},{5,4},{6,5},{7,6},{8,7},{9,8},{10,9... | collective-permute-start | bytes 73736 | tf_op jit(solution)/shard_map/ppermute | solution.py:32
  43.7 0.6 collective-permute-done.10
  44.4 0.2 collective-permute-done.11
  44.5 3.6 %collective-permute-start.13 = (bf16[32,384]{1,0:T(8,128)(2,1)S(1)}, bf16[32,384]{1,0:T(8,128)(2,1)S(1)}, u32[]{:S(2)}, u32[]{:S(2)}) collective-permute-start(bf16[32,384]{1,0:T(8,128)(2,1)S(1)} %collective-permute-done.11), channel_id=1, source_target_pairs={{0,15},{1,0},{2,1},{3,2},{4,3},{5,4},{6,5},{7,6},{8,7},{9,8},{10,9... | collective-permute-start | bytes 73736 | tf_op jit(solution)/shard_map/ppermute | solution.py:32
  48.2 0.6 collective-permute-done.12
  48.8 0.2 collective-permute-done.13
  49.0 3.6 %collective-permute-start.15 = (bf16[32,384]{1,0:T(8,128)(2,1)S(1)}, bf16[32,384]{1,0:T(8,128)(2,1)S(1)}, u32[]{:S(2)}, u32[]{:S(2)}) collective-permute-start(bf16[32,384]{1,0:T(8,128)(2,1)S(1)} %collective-permute-done.13), channel_id=1, source_target_pairs={{0,15},{1,0},{2,1},{3,2},{4,3},{5,4},{6,5},{7,6},{8,7},{9,8},{10,9... | collective-permute-start | bytes 73736 | tf_op jit(solution)/shard_map/ppermute | solution.py:32
  52.6 0.6 collective-permute-done.14
  53.3 0.2 collective-permute-done.15
  53.5 4.3 %collective-permute-done.16 = bf16[32,384]{1,0:T(8,128)(2,1)S(1)} collective-permute-done((bf16[32,384]{1,0:T(8,128)(2,1)S(1)}, bf16[32,384]{1,0:T(8,128)(2,1)S(1)}, u32[]{:S(2)}, u32[]{:S(2)}) %collective-permute-start.16) | collective-permute-done | bytes 24608 | tf_op jit(solution)/shard_map/ppermute | solution.py:26
  57.8 1.2 multiply_reduce_fusion.1
  59.0 0.6 broadcast_in_dim.42
  59.6 7.6 %all-to-all-start = ((f32[16,1,384]{2,1,0:T(1,128)}), f32[16,1,384]{2,1,0:T(1,128)S(1)}, u32[]{:S(2)}, u32[]{:S(2)}) async-start(f32[16,1,384]{2,1,0:T(1,128)} %broadcast_in_dim.42), calls=%async_computation | async-start | bytes 49152 | tf_op jit(solution)/shard_map/all_to_all | solution.py:57
  67.3 0.7 convert_element_type.68
  68.0 6.6 %all-to-all-done = f32[16,1,384]{2,1,0:T(1,128)S(1)} async-done(((f32[16,1,384]{2,1,0:T(1,128)}), f32[16,1,384]{2,1,0:T(1,128)S(1)}, u32[]{:S(2)}, u32[]{:S(2)}) %all-to-all-start) | async-done | bytes 24608 | tf_op jit(solution)/shard_map/all_to_all | solution.py:57
  74.9 3.2 %gather_fusion = bf16[1536,128]{1,0:T(8,128)(2,1)S(1)} fusion(bf16[384,128]{1,0:T(8,128)(2,1)S(1)} %copy.69, s32[2048]{0:T(1024)S(1)} %pad_clamp_fusion), kind=kCustom, calls=%fused_computation | custom fusion | bytes 792576 | tf_op jit(solution)/shard_map/gather | solution.py:134
  78.1 0.3 broadcast_select_fusion
  78.4 28.7 %all_to_all.27 = bf16[32,48,128]{2,1,0:T(8,128)(2,1)} all-to-all(bf16[32,48,128]{2,1,0:T(8,128)(2,1)S(1)} %broadcast_select_fusion), channel_id=1, replica_groups=mesh['sp'=32,'tp'=16] {'sp'}, dimensions={0} | all-to-all | bytes 786432 | tf_op jit(solution)/shard_map/all_to_all | solution.py:137
  107.1 52.3 %all-gather.4.cloned.1.call-done = bf16[1,1536,2048]{2,1,0:T(8,128)(2,1)} async-done(((bf16[1,1536,128]{2,1,0:T(8,128)(2,1)}), bf16[1,1536,2048]{2,1,0:T(8,128)(2,1)}) %all-gather.4.cloned.1.call-update) | async-done | bytes 6291472 | tf_op jit(solution)/shard_map/all_gather | solution.py:138
  159.4 3.4 %copy.70 = bf16[2,32,24,2048]{3,2,1,0:T(8,128)(2,1)S(1)} copy(bf16[2,32,24,2048]{3,2,0,1:T(8,128)(2,1)} %bitcast.62) | data formatting | bytes 12582912 | tf_op jit(solution)/shard_map/transpose | solution.py:141
  162.8 1.8 fusion.21
  164.7 2.6 fusion
  167.3 0.2 all-gather.8.cloned.1.call-start
  167.5 0.5 all-gather.8.cloned.1.call-update
  168.2 58.0 %all-gather.6.cloned.1.call-done = bf16[2,768,2048]{2,1,0:T(8,128)(2,1)} async-done(((bf16[2,768,128]{2,1,0:T(8,128)(2,1)}), bf16[2,768,2048]{2,1,0:T(8,128)(2,1)}) %all-gather.6.cloned.1.call-update) | async-done | bytes 6291472 | tf_op jit(solution)/shard_map/all_gather | solution.py:150
  226.3 4.6 %convolution_convert_fusion = bf16[2,768,128]{2,1,0:T(8,128)(2,1)S(1)} fusion(bf16[2,768,2048]{2,1,0:T(8,128)(2,1)} %all-gather.6.cloned.1.call-done, bf16[2,2048,128]{2,1,0:T(8,128)(2,1)S(1)} %copy-done.7), kind=kOutput, calls=%fused_computation.5 | convolution fusion | flops 805502976 | bytes 7733248 | tf_op jit(solution)/shard_map/erf,efd->erd/dot_general | solution.py:148
  230.9 6.1 %copy.88 = bf16[1,1536,128]{2,0,1:T(2,128)(2,1)S(1)} copy(bf16[1,1536,128]{2,1,0:T(8,128)(2,1)S(1)} %bitcast.67) | data formatting | bytes 786432 | tf_op jit(solution)/shard_map/reshape | solution.py:158
  237.0 0.6 broadcast.108
  237.6 8.8 %reduce.7 = bf16[1536,128]{1,0:T(8,128)(2,1)S(1)} reduce(bf16[1536,1,128]{2,1,0:T(2,128)(2,1)S(1)} %bitcast.63, bf16[]{:T(256)} %broadcast.108), dimensions={1}, to_apply=%bitcast.56.reduce_sub_computation | reduce | bytes 786434
  246.4 0.8 reshape.133
  247.2 9.9 %all-to-all-start.2 = ((bf16[32,2,3072]{2,1,0:T(2,128)(2,1)}), bf16[32,2,3072]{2,1,0:T(2,128)(2,1)S(1)}, u32[]{:S(2)}, u32[]{:S(2)}) async-start(bf16[32,2,3072]{2,1,0:T(2,128)(2,1)} %reshape.133), calls=%async_computation.2 | async-start | bytes 786432 | tf_op jit(solution)/shard_map/all_to_all | solution.py:160
  257.3 11.8 %all-gather.8.cloned.1.call-done = bf16[384,2048]{0,1:T(8,128)(2,1)} async-done(((bf16[384,128]{0,1:T(8,128)(2,1)}), bf16[384,2048]{0,1:T(8,128)(2,1)}) %all-gather.8.cloned.1.call-update) | async-done | bytes 1572880 | tf_op jit(solution)/shard_map/all_gather | solution.py:116
  269.1 1.7 fusion.22
  270.9 1.8 fusion.4
  272.6 16.9 %all_gather.15 = bf16[384,512]{0,1:T(8,128)(2,1)S(1)} all-gather(bf16[384,32]{0,1:T(8,128)(2,1)S(1)} %fusion.4), channel_id=1, replica_groups=mesh['sp'=32,'tp'=16] {'tp'}, dimensions={1}, use_global_device_ids=true | all-gather | bytes 417792 | tf_op jit(solution)/shard_map/all_gather | solution.py:123
  289.5 0.3 reshape.134
  289.9 1.9 gather_fusion.1
  291.8 0.6 multiply_reduce_fusion
  292.5 0.3 fusion.3
  292.8 0.8 copy.74
  (74 shorter events, 1.9 us)
Async XLA Ops:
  6.5 156.3 %copy-start = (bf16[2,2048,128]{2,1,0:T(8,128)(2,1)S(1)}, bf16[2,2048,128]{2,1,0:T(8,128)(2,1)}, u32[]{:S(2)}) copy-start(bf16[2,2048,128]{2,1,0:T(8,128)(2,1)} %param.24) | copy-start | bytes 3145732
  7.5 13.1 %collective-permute-start = (bf16[32,1]{1,0:T(8,128)(2,1)S(1)}, bf16[32,1]{1,0:T(8,128)(2,1)S(1)}, u32[]{:S(2)}, u32[]{:S(2)}) collective-permute-start(bf16[32,1]{1,0:T(8,128)(2,1)S(1)} %get-tuple-element.9), channel_id=1, source_target_pairs={{0,16},{16,32},{32,48},{48,64},{64,80},{80,96},{96,112},{112,128},... | collective-permute-start | bytes 200 | tf_op jit(solution)/shard_map/ppermute | solution.py:49
  11.4 9.2 %collective-permute-start.1 = (bf16[32,1]{1,0:T(8,128)(2,1)S(1)}, bf16[32,1]{1,0:T(8,128)(2,1)S(1)}, u32[]{:S(2)}, u32[]{:S(2)}) collective-permute-start(bf16[32,1]{1,0:T(8,128)(2,1)S(1)} %get-tuple-element.10), channel_id=1, source_target_pairs={{16,0},{32,16},{48,32},{64,48},{80,64},{96,80},{112,96},{128,112},... | collective-permute-start | bytes 200 | tf_op jit(solution)/shard_map/ppermute | solution.py:50
  21.6 5.3 %collective-permute-start.2 = (bf16[32,384]{1,0:T(8,128)(2,1)S(1)}, bf16[32,384]{1,0:T(8,128)(2,1)S(1)}, u32[]{:S(2)}, u32[]{:S(2)}) collective-permute-start(bf16[32,384]{1,0:T(8,128)(2,1)S(1)} %get-tuple-element.6), channel_id=1, source_target_pairs={{0,1},{1,2},{2,3},{3,4},{4,5},{5,6},{6,7},{7,8},{8,9},{9,10},{10,1... | collective-permute-start | bytes 73736 | tf_op jit(solution)/shard_map/ppermute | solution.py:26
  23.8 3.3 %collective-permute-start.3 = (bf16[32,384]{1,0:T(8,128)(2,1)S(1)}, bf16[32,384]{1,0:T(8,128)(2,1)S(1)}, u32[]{:S(2)}, u32[]{:S(2)}) collective-permute-start(bf16[32,384]{1,0:T(8,128)(2,1)S(1)} %get-tuple-element.6), channel_id=1, source_target_pairs={{0,15},{1,0},{2,1},{3,2},{4,3},{5,4},{6,5},{7,6},{8,7},{9,8},{10,9... | collective-permute-start | bytes 73736 | tf_op jit(solution)/shard_map/ppermute | solution.py:32
  27.0 4.0 %collective-permute-start.4 = (bf16[32,384]{1,0:T(8,128)(2,1)S(1)}, bf16[32,384]{1,0:T(8,128)(2,1)S(1)}, u32[]{:S(2)}, u32[]{:S(2)}) collective-permute-start(bf16[32,384]{1,0:T(8,128)(2,1)S(1)} %collective-permute-done.2), channel_id=1, source_target_pairs={{0,1},{1,2},{2,3},{3,4},{4,5},{5,6},{6,7},{7,8},{8,9},{9,10},{10,1... | collective-permute-start | bytes 73736 | tf_op jit(solution)/shard_map/ppermute | solution.py:26
  27.0 4.1 %collective-permute-start.5 = (bf16[32,384]{1,0:T(8,128)(2,1)S(1)}, bf16[32,384]{1,0:T(8,128)(2,1)S(1)}, u32[]{:S(2)}, u32[]{:S(2)}) collective-permute-start(bf16[32,384]{1,0:T(8,128)(2,1)S(1)} %collective-permute-done.3), channel_id=1, source_target_pairs={{0,15},{1,0},{2,1},{3,2},{4,3},{5,4},{6,5},{7,6},{8,7},{9,8},{10,9... | collective-permute-start | bytes 73736 | tf_op jit(solution)/shard_map/ppermute | solution.py:32
  31.0 4.5 %collective-permute-start.6 = (bf16[32,384]{1,0:T(8,128)(2,1)S(1)}, bf16[32,384]{1,0:T(8,128)(2,1)S(1)}, u32[]{:S(2)}, u32[]{:S(2)}) collective-permute-start(bf16[32,384]{1,0:T(8,128)(2,1)S(1)} %collective-permute-done.4), channel_id=1, source_target_pairs={{0,1},{1,2},{2,3},{3,4},{4,5},{5,6},{6,7},{7,8},{8,9},{9,10},{10,1... | collective-permute-start | bytes 73736 | tf_op jit(solution)/shard_map/ppermute | solution.py:26
  31.2 4.5 %collective-permute-start.7 = (bf16[32,384]{1,0:T(8,128)(2,1)S(1)}, bf16[32,384]{1,0:T(8,128)(2,1)S(1)}, u32[]{:S(2)}, u32[]{:S(2)}) collective-permute-start(bf16[32,384]{1,0:T(8,128)(2,1)S(1)} %collective-permute-done.5), channel_id=1, source_target_pairs={{0,15},{1,0},{2,1},{3,2},{4,3},{5,4},{6,5},{7,6},{8,7},{9,8},{10,9... | collective-permute-start | bytes 73736 | tf_op jit(solution)/shard_map/ppermute | solution.py:32
  35.4 4.5 %collective-permute-start.8 = (bf16[32,384]{1,0:T(8,128)(2,1)S(1)}, bf16[32,384]{1,0:T(8,128)(2,1)S(1)}, u32[]{:S(2)}, u32[]{:S(2)}) collective-permute-start(bf16[32,384]{1,0:T(8,128)(2,1)S(1)} %collective-permute-done.6), channel_id=1, source_target_pairs={{0,1},{1,2},{2,3},{3,4},{4,5},{5,6},{6,7},{7,8},{8,9},{9,10},{10,1... | collective-permute-start | bytes 73736 | tf_op jit(solution)/shard_map/ppermute | solution.py:26
  35.6 4.5 %collective-permute-start.9 = (bf16[32,384]{1,0:T(8,128)(2,1)S(1)}, bf16[32,384]{1,0:T(8,128)(2,1)S(1)}, u32[]{:S(2)}, u32[]{:S(2)}) collective-permute-start(bf16[32,384]{1,0:T(8,128)(2,1)S(1)} %collective-permute-done.7), channel_id=1, source_target_pairs={{0,15},{1,0},{2,1},{3,2},{4,3},{5,4},{6,5},{7,6},{8,7},{9,8},{10,9... | collective-permute-start | bytes 73736 | tf_op jit(solution)/shard_map/ppermute | solution.py:32
  39.9 4.5 %collective-permute-start.10 = (bf16[32,384]{1,0:T(8,128)(2,1)S(1)}, bf16[32,384]{1,0:T(8,128)(2,1)S(1)}, u32[]{:S(2)}, u32[]{:S(2)}) collective-permute-start(bf16[32,384]{1,0:T(8,128)(2,1)S(1)} %collective-permute-done.8), channel_id=1, source_target_pairs={{0,1},{1,2},{2,3},{3,4},{4,5},{5,6},{6,7},{7,8},{8,9},{9,10},{10,1... | collective-permute-start | bytes 73736 | tf_op jit(solution)/shard_map/ppermute | solution.py:26
  40.1 4.5 %collective-permute-start.11 = (bf16[32,384]{1,0:T(8,128)(2,1)S(1)}, bf16[32,384]{1,0:T(8,128)(2,1)S(1)}, u32[]{:S(2)}, u32[]{:S(2)}) collective-permute-start(bf16[32,384]{1,0:T(8,128)(2,1)S(1)} %collective-permute-done.9), channel_id=1, source_target_pairs={{0,15},{1,0},{2,1},{3,2},{4,3},{5,4},{6,5},{7,6},{8,7},{9,8},{10,9... | collective-permute-start | bytes 73736 | tf_op jit(solution)/shard_map/ppermute | solution.py:32
  44.4 4.5 %collective-permute-start.12 = (bf16[32,384]{1,0:T(8,128)(2,1)S(1)}, bf16[32,384]{1,0:T(8,128)(2,1)S(1)}, u32[]{:S(2)}, u32[]{:S(2)}) collective-permute-start(bf16[32,384]{1,0:T(8,128)(2,1)S(1)} %collective-permute-done.10), channel_id=1, source_target_pairs={{0,1},{1,2},{2,3},{3,4},{4,5},{5,6},{6,7},{7,8},{8,9},{9,10},{10,1... | collective-permute-start | bytes 73736 | tf_op jit(solution)/shard_map/ppermute | solution.py:26
  44.5 4.5 %collective-permute-start.13 = (bf16[32,384]{1,0:T(8,128)(2,1)S(1)}, bf16[32,384]{1,0:T(8,128)(2,1)S(1)}, u32[]{:S(2)}, u32[]{:S(2)}) collective-permute-start(bf16[32,384]{1,0:T(8,128)(2,1)S(1)} %collective-permute-done.11), channel_id=1, source_target_pairs={{0,15},{1,0},{2,1},{3,2},{4,3},{5,4},{6,5},{7,6},{8,7},{9,8},{10,9... | collective-permute-start | bytes 73736 | tf_op jit(solution)/shard_map/ppermute | solution.py:32
  48.8 4.5 %collective-permute-start.14 = (bf16[32,384]{1,0:T(8,128)(2,1)S(1)}, bf16[32,384]{1,0:T(8,128)(2,1)S(1)}, u32[]{:S(2)}, u32[]{:S(2)}) collective-permute-start(bf16[32,384]{1,0:T(8,128)(2,1)S(1)} %collective-permute-done.12), channel_id=1, source_target_pairs={{0,1},{1,2},{2,3},{3,4},{4,5},{5,6},{6,7},{7,8},{8,9},{9,10},{10,1... | collective-permute-start | bytes 73736 | tf_op jit(solution)/shard_map/ppermute | solution.py:26
  49.0 4.5 %collective-permute-start.15 = (bf16[32,384]{1,0:T(8,128)(2,1)S(1)}, bf16[32,384]{1,0:T(8,128)(2,1)S(1)}, u32[]{:S(2)}, u32[]{:S(2)}) collective-permute-start(bf16[32,384]{1,0:T(8,128)(2,1)S(1)} %collective-permute-done.13), channel_id=1, source_target_pairs={{0,15},{1,0},{2,1},{3,2},{4,3},{5,4},{6,5},{7,6},{8,7},{9,8},{10,9... | collective-permute-start | bytes 73736 | tf_op jit(solution)/shard_map/ppermute | solution.py:32
  53.3 4.5 %collective-permute-start.16 = (bf16[32,384]{1,0:T(8,128)(2,1)S(1)}, bf16[32,384]{1,0:T(8,128)(2,1)S(1)}, u32[]{:S(2)}, u32[]{:S(2)}) collective-permute-start(bf16[32,384]{1,0:T(8,128)(2,1)S(1)} %collective-permute-done.14), channel_id=1, source_target_pairs={{0,1},{1,2},{2,3},{3,4},{4,5},{5,6},{6,7},{7,8},{8,9},{9,10},{10,1... | collective-permute-start | bytes 73736 | tf_op jit(solution)/shard_map/ppermute | solution.py:26
  59.6 15.0 %all-to-all-start = ((f32[16,1,384]{2,1,0:T(1,128)}), f32[16,1,384]{2,1,0:T(1,128)S(1)}, u32[]{:S(2)}, u32[]{:S(2)}) async-start(f32[16,1,384]{2,1,0:T(1,128)} %broadcast_in_dim.42), calls=%async_computation | async-start | bytes 49152 | tf_op jit(solution)/shard_map/all_to_all | solution.py:57
  67.2 92.2 %all-gather.4.cloned.1.call-start = ((), (), s32[]{:S(2)}) async-start(), calls=%async_computation.3 | async-start | bytes 6684672 | tf_op jit(solution)/shard_map/all_gather | solution.py:138
  74.8 88.0 %copy-start.1 = (bf16[384,128]{0,1:T(8,128)(2,1)}, bf16[384,128]{0,1:T(8,128)(2,1)S(1)}, u32[]{:S(2)}) copy-start(bf16[384,128]{0,1:T(8,128)(2,1)S(1)} %multiply_convert_fusion) | copy-start | bytes 294916
  107.1 119.2 %all-gather.6.cloned.1.call-start = ((), (), s32[]{:S(2)}) async-start(), calls=%async_computation.4 | async-start | bytes 6684672 | tf_op jit(solution)/shard_map/all_gather | solution.py:150
  162.8 1.8 copy-start.6
  164.6 3.4 %copy-start.5 = (f32[384,2]{0,1:T(2,128)S(1)}, f32[384,2]{0,1:T(2,128)}, u32[]{:S(2)}) copy-start(f32[384,2]{0,1:T(2,128)} %param.23) | copy-start | bytes 9220
  164.6 61.6 %copy-start.7 = (bf16[2,2048,128]{2,1,0:T(8,128)(2,1)S(1)}, bf16[2,2048,128]{2,1,0:T(8,128)(2,1)}, u32[]{:S(2)}) copy-start(bf16[2,2048,128]{2,1,0:T(8,128)(2,1)} %param.26) | copy-start | bytes 3145732
  167.3 101.8 %all-gather.8.cloned.1.call-start = ((), (), s32[]{:S(2)}) async-start(), calls=%async_computation.5 | async-start | bytes 1671168 | tf_op jit(solution)/shard_map/all_gather | solution.py:116
  168.2 100.9 %copy-start.3 = (bf16[2048,32]{0,1:T(8,128)(2,1)S(1)}, bf16[2048,32]{0,1:T(8,128)(2,1)}, u32[]{:S(2)}) copy-start(bf16[2048,32]{0,1:T(8,128)(2,1)} %param.27) | copy-start | bytes 393220
  168.2 102.6 %copy-start.2 = (bf16[2048,32]{0,1:T(8,128)(2,1)S(1)}, bf16[2048,32]{0,1:T(8,128)(2,1)}, u32[]{:S(2)}) copy-start(bf16[2048,32]{0,1:T(8,128)(2,1)} %param.28) | copy-start | bytes 393220
  237.0 55.5 %copy-start.4 = (bf16[512,128]{1,0:T(8,128)(2,1)S(1)}, bf16[512,128]{1,0:T(8,128)(2,1)}, u32[]{:S(2)}) copy-start(bf16[512,128]{1,0:T(8,128)(2,1)} %param.29) | copy-start | bytes 393220
  247.2 42.3 %all-to-all-start.2 = ((bf16[32,2,3072]{2,1,0:T(2,128)(2,1)}), bf16[32,2,3072]{2,1,0:T(2,128)(2,1)S(1)}, u32[]{:S(2)}, u32[]{:S(2)}) async-start(bf16[32,2,3072]{2,1,0:T(2,128)(2,1)} %reshape.133), calls=%async_computation.2 | async-start | bytes 786432 | tf_op jit(solution)/shard_map/all_to_all | solution.py:160
Sparse Core Ops, SparseCore 0:
  107.2 52.1 all-gather.3
  167.4 58.8 all-gather.5
  228.4 40.6 all-gather.7
